TPU v7x, 32 devices: a whole 2x2x4 slice. The times are simulated.
32 devices in a mesh: sp: 8 (over z, y), tp: 4 (over x, core).
Axes of the slice: x: 2, y: 2, z: 4, core: 2. Of those that a mesh axis runs over, the one named last changes fastest.
Arguments:
- stream: bfloat16 [2048, 2048], P('sp', 'tp'), may hold values from -6 to 6
- norm_gain: float32 [2, 2048], replicated, may hold values from 0.1 to 1.9
- w_value: bfloat16 [2, 2048, 1024], P(None, 'sp', 'tp'), may hold values from -0.125 to 0.125
- w_gate: bfloat16 [2, 2048, 1024], P(None, 'sp', 'tp'), may hold values from -0.125 to 0.125
- conv_taps: float32 [2, 128, 1024], P(None, None, 'tp'), as said below
- channel_gain: float32 [2, 1024], P(None, 'tp'), may hold values from 0.1 to 1.9
- w_out: bfloat16 [2, 1024, 2048], P(None, 'tp', 'sp'), may hold values from -0.1875 to 0.1875
Outputs:
- result: bfloat16 [2048, 2048], P('sp', 'tp')
Inputs may be any that keep to these rules, and one draw needn't show every extreme that they name: `conv_taps`: taps of each block of 128 consecutive channels share a scale factor of its own.
All inputs are finite; a program needn't handle non-finite values.
Results may differ from a plain program's by a relative error of at most 0.012.
Values may be sent and summed in bfloat16 or wider, within the bound.
A program may use at most 64 MiB of HBM per device.

v0:
```python
import jax
import jax.numpy as jnp
from jax import lax
from jax.sharding import PartitionSpec as P

C = 1024
LAYERS = 2


def from_behind(value, axis, steps):
    count = lax.axis_size(axis)
    initial, last = (max(0, -steps), min(count, count - steps))
    return lax.ppermute(value, axis, [(source, source + steps) for source in range(initial, last)])


def shards(stream, norm_gain, w_value, w_gate, conv_taps, channel_gain, w_out):
    x = stream
    tokens_here = stream.shape[0]
    local_ch = w_value.shape[2]
    taps = conv_taps.shape[1]
    for layer in range(LAYERS):
        whole = lax.all_gather(x, "tp", axis=1, tiled=True).astype(jnp.float32)
        normed = (
            whole
            * lax.rsqrt(jnp.mean(whole * whole, axis=1, keepdims=True) + 1e-06)
            * norm_gain[layer]
        ).astype(jnp.bfloat16)
        value_whole, gate_whole = (
            lax.all_gather(w_value[layer], "sp", axis=0, tiled=True),
            lax.all_gather(w_gate[layer], "sp", axis=0, tiled=True),
        )
        value = jnp.dot(normed, value_whole, preferred_element_type=jnp.float32)
        gate = jnp.dot(normed, gate_whole, preferred_element_type=jnp.float32)
        glu = (value * jax.nn.sigmoid(gate)).astype(jnp.bfloat16)
        before = from_behind(glu[tokens_here - taps :], "sp", 1)
        padded = jnp.concatenate([before[1:], glu], axis=0).astype(jnp.float32)
        conv = lax.conv_general_dilated(
            padded[None],
            conv_taps[layer][:, None, :],
            (1,),
            "VALID",
            dimension_numbers=("NWC", "WIO", "NWC"),
            feature_group_count=local_ch,
            precision=lax.Precision.HIGHEST,
        )[0]
        mean = lax.psum(jnp.sum(conv, axis=1, keepdims=True), "tp") / C
        centred = conv - mean
        spread = lax.psum(jnp.sum(centred * centred, axis=1, keepdims=True), "tp") / C
        act = jax.nn.silu(centred * lax.rsqrt(spread + 1e-05) * channel_gain[layer]).astype(
            jnp.bfloat16
        )
        out_whole = lax.all_gather(w_out[layer], "sp", axis=1, tiled=True)
        terms = jnp.dot(act, out_whole, preferred_element_type=jnp.float32)
        branch = lax.psum_scatter(terms, "tp", scatter_dimension=1, tiled=True)
        x = (x.astype(jnp.float32) + branch).astype(jnp.bfloat16)
    return x


def solution(mesh):
    return jax.shard_map(
        shards,
        mesh=mesh,
        in_specs=(
            P("sp", "tp"),
            P(),
            P(None, "sp", "tp"),
            P(None, "sp", "tp"),
            P(None, None, "tp"),
            P(None, "tp"),
            P(None, "tp", "sp"),
        ),
        out_specs=P("sp", "tp"),
        check_vma=False,
    )
```

profile of v0, /device:TPU:0, one launch (start us, length us, event | category | flops | bytes accessed | tf_op | source)
XLA Modules:
  0.0 370.0 jit_solution(6867189528916284857)
XLA Ops:
  12.7 15.7 %all-gather.15.cloned.1.call-done = bf16[256,2048]{1,0:T(8,128)(2,1)} async-done(((bf16[256,512]{1,0:T(8,128)(2,1)}), bf16[256,2048]{1,0:T(8,128)(2,1)}) %all-gather.15.cloned.1.call-update) | async-done | bytes 1048592 | tf_op jit(solution)/shard_map/all_gather | solution.py:22
  30.0 40.8 %all-gather.19.cloned.1.call-done = bf16[1,2048,256]{2,1,0:T(8,128)(2,1)} async-done(((bf16[1,256,256]{2,1,0:T(8,128)(2,1)}), bf16[1,2048,256]{2,1,0:T(8,128)(2,1)}) %all-gather.19.cloned.1.call-update) | async-done | bytes 1048592 | tf_op jit(solution)/shard_map/all_gather | solution.py:29
  70.8 2.0 fusion.24
  72.8 39.1 %all-gather.21.cloned.1.call-done = bf16[1,2048,256]{2,1,0:T(8,128)(2,1)} async-done(((bf16[1,256,256]{2,1,0:T(8,128)(2,1)}), bf16[1,2048,256]{2,1,0:T(8,128)(2,1)}) %all-gather.21.cloned.1.call-update) | async-done | bytes 1048592 | tf_op jit(solution)/shard_map/all_gather | solution.py:30
  113.7 2.5 collective-permute-start
  116.2 1.9 collective-permute-done
  118.1 4.8 %fusion.50 = (f32[256]{0:T(256)S(1)}, f32[1,256,256]{2,0,1:T(1,128)S(1)}) fusion(f32[1,128,256]{2,1,0:T(8,128)S(1)} %get-tuple-element.6, bf16[1,383,256]{2,1,0:T(8,128)(2,1)S(1)} %maximum_bitcast_fusion), kind=kOutput, calls=%fused_computation.70 | convolution fusion | flops 100728576 | bytes 590336 | tf_op jit(solution)/shard_map/conv_general_dilated | solution.py:37
  123.0 5.7 %psum.28 = f32[256,1]{0,1:T(1,128)S(1)} all-reduce(f32[256,1]{0,1:T(1,128)S(1)} %bitcast.72), channel_id=1, replica_groups=mesh['sp'=8,'tp'=4] {'tp'}, use_global_device_ids=true, to_apply=%region_2.0 | all-reduce | flops 256 | bytes 2048 | tf_op jit(solution)/shard_map/psum | solution.py:46
  128.8 7.0 %psum.29 = f32[256,1]{0,1:T(1,128)S(1)} all-reduce(f32[256,1]{0,1:T(1,128)S(1)} %bitcast.68), channel_id=1, replica_groups=mesh['sp'=8,'tp'=4] {'tp'}, use_global_device_ids=true, to_apply=%region_4.0 | all-reduce | flops 256 | bytes 2048 | tf_op jit(solution)/shard_map/psum | solution.py:48
  135.8 16.2 %all-gather.23.cloned.1.call-done = bf16[1,256,2048]{2,1,0:T(8,128)(2,1)} async-done(((bf16[1,256,256]{2,1,0:T(8,128)(2,1)}), bf16[1,256,2048]{2,1,0:T(8,128)(2,1)}) %all-gather.23.cloned.1.call-update) | async-done | bytes 1048592 | tf_op jit(solution)/shard_map/all_gather | solution.py:52
  152.0 3.1 fusion.21
  155.2 30.3 %reduce-scatter.3.cloned.1.call-done = f32[256,512]{1,0:T(8,128)} async-done(((f32[256,2048]{1,0:T(8,128)}), f32[256,512]{1,0:T(8,128)}) %reduce-scatter.3.cloned.1.call-update) | async-done | bytes 524304 | tf_op jit(solution)/shard_map/reduce_scatter | solution.py:54
  189.6 14.6 %all-gather.17.cloned.1.call-done = bf16[256,2048]{1,0:T(8,128)(2,1)} async-done(((bf16[256,512]{1,0:T(8,128)(2,1)}), bf16[256,2048]{1,0:T(8,128)(2,1)}) %all-gather.17.cloned.1.call-update) | async-done | bytes 1048592 | tf_op jit(solution)/shard_map/all_gather | solution.py:22
  205.8 40.8 %all-gather.25.cloned.1.call-done = bf16[1,2048,256]{2,1,0:T(8,128)(2,1)} async-done(((bf16[1,256,256]{2,1,0:T(8,128)(2,1)}), bf16[1,2048,256]{2,1,0:T(8,128)(2,1)}) %all-gather.25.cloned.1.call-update) | async-done | bytes 1048592 | tf_op jit(solution)/shard_map/all_gather | solution.py:29
  246.6 2.0 fusion.19
  248.6 39.1 %all-gather.27.cloned.1.call-done = bf16[1,2048,256]{2,1,0:T(8,128)(2,1)} async-done(((bf16[1,256,256]{2,1,0:T(8,128)(2,1)}), bf16[1,2048,256]{2,1,0:T(8,128)(2,1)}) %all-gather.27.cloned.1.call-update) | async-done | bytes 1048592 | tf_op jit(solution)/shard_map/all_gather | solution.py:30
  289.5 2.5 collective-permute-start.1
  292.0 1.9 collective-permute-done.1
  293.9 4.8 %fusion.51 = (f32[256]{0:T(256)S(1)}, f32[1,256,256]{2,0,1:T(1,128)S(1)}) fusion(f32[1,128,256]{2,1,0:T(8,128)S(1)} %get-tuple-element.5, bf16[1,383,256]{2,1,0:T(8,128)(2,1)S(1)} %maximum_bitcast_fusion.1), kind=kOutput, calls=%fused_computation.71 | convolution fusion | flops 100728576 | bytes 590336 | tf_op jit(solution)/shard_map/conv_general_dilated | solution.py:37
  298.8 5.7 %psum.30 = f32[256,1]{0,1:T(1,128)S(1)} all-reduce(f32[256,1]{0,1:T(1,128)S(1)} %bitcast.73), channel_id=1, replica_groups=mesh['sp'=8,'tp'=4] {'tp'}, use_global_device_ids=true, to_apply=%region_8.9 | all-reduce | flops 256 | bytes 2048 | tf_op jit(solution)/shard_map/psum | solution.py:46
  304.6 7.0 %psum.31 = f32[256,1]{0,1:T(1,128)S(1)} all-reduce(f32[256,1]{0,1:T(1,128)S(1)} %bitcast.69), channel_id=1, replica_groups=mesh['sp'=8,'tp'=4] {'tp'}, use_global_device_ids=true, to_apply=%region_10.11 | all-reduce | flops 256 | bytes 2048 | tf_op jit(solution)/shard_map/psum | solution.py:48
  311.6 16.3 %all-gather.29.cloned.1.call-done = bf16[1,256,2048]{2,1,0:T(8,128)(2,1)} async-done(((bf16[1,256,256]{2,1,0:T(8,128)(2,1)}), bf16[1,256,2048]{2,1,0:T(8,128)(2,1)}) %all-gather.29.cloned.1.call-update) | async-done | bytes 1048592 | tf_op jit(solution)/shard_map/all_gather | solution.py:52
  327.9 3.1 fusion.16
  331.1 30.3 %reduce-scatter.5.cloned.1.call-done = f32[256,512]{1,0:T(8,128)} async-done(((f32[256,2048]{1,0:T(8,128)}), f32[256,512]{1,0:T(8,128)}) %reduce-scatter.5.cloned.1.call-update) | async-done | bytes 524304 | tf_op jit(solution)/shard_map/reduce_scatter | solution.py:54
  (60 shorter events, 19.2 us)
Async XLA Ops:
  6.5 6.1 %copy-start.5 = (f32[2,2048]{1,0:T(2,128)S(1)}, f32[2,2048]{1,0:T(2,128)}, u32[]{:S(2)}) copy-start(f32[2,2048]{1,0:T(2,128)} %param.8) | copy-start | bytes 49156
  6.5 6.1 %copy-start.4 = (f32[2,128,256]{2,1,0:T(8,128)S(1)}, f32[2,128,256]{2,1,0:T(8,128)}, u32[]{:S(2)}) copy-start(f32[2,128,256]{2,1,0:T(8,128)} %param.11) | copy-start | bytes 786436
  6.5 21.8 %all-gather.15.cloned.1.call-start = ((), (), s32[]{:S(2)}) async-start(), calls=%async_computation.2 | async-start | bytes 1310720 | tf_op jit(solution)/shard_map/all_gather | solution.py:22
  7.3 63.5 %all-gather.19.cloned.1.call-start = ((), (), s32[]{:S(2)}) async-start(), calls=%async_computation.6 | async-start | bytes 1179648 | tf_op jit(solution)/shard_map/all_gather | solution.py:29
  9.0 102.9 %all-gather.21.cloned.1.call-start = ((), (), s32[]{:S(2)}) async-start(), calls=%async_computation.7 | async-start | bytes 1179648 | tf_op jit(solution)/shard_map/all_gather | solution.py:30
  10.8 141.2 %all-gather.23.cloned.1.call-start = ((), (), s32[]{:S(2)}) async-start(), calls=%async_computation.8 | async-start | bytes 1179648 | tf_op jit(solution)/shard_map/all_gather | solution.py:52
  12.6 172.9 %reduce-scatter.3.cloned.1.call-start = ((), (), s32[]{:S(2)}) async-start(), calls=%async_computation.3 | async-start | bytes 2621440 | tf_op jit(solution)/shard_map/reduce_scatter | solution.py:54
  28.4 83.6 %copy-start.1 = (bf16[256,2048]{1,0:T(8,128)(2,1)S(1)}, bf16[256,2048]{1,0:T(8,128)(2,1)}, u32[]{:S(2)}) copy-start(bf16[256,2048]{1,0:T(8,128)(2,1)} %all-gather.15.cloned.1.call-done) | copy-start | bytes 3145732
  72.8 43.4 %copy-start.6 = (f32[2,256]{1,0:T(2,128)S(1)}, f32[2,256]{1,0:T(2,128)}, u32[]{:S(2)}) copy-start(f32[2,256]{1,0:T(2,128)} %param.12) | copy-start | bytes 6148
  113.7 4.4 %collective-permute-start = (bf16[128,256]{1,0:T(8,128)(2,1)S(1)}, bf16[128,256]{1,0:T(8,128)(2,1)S(1)}, u32[]{:S(2)}, u32[]{:S(2)}) collective-permute-start(bf16[128,256]{1,0:T(8,128)(2,1)S(1)} %slice.64), channel_id=1, source_target_pairs={{0,4},{4,8},{8,12},{12,16},{16,20},{20,24},{24,28},{1,5},{5,9},{9,... | collective-permute-start | bytes 196616 | tf_op jit(solution)/shard_map/ppermute | solution.py:13
  152.0 33.5 %copy-start.3 = (bf16[256,512]{1,0:T(8,128)(2,1)S(1)}, bf16[256,512]{1,0:T(8,128)(2,1)}, u32[]{:S(2)}) copy-start(bf16[256,512]{1,0:T(8,128)(2,1)} %param.7) | copy-start | bytes 786436
  155.1 49.0 %all-gather.17.cloned.1.call-start = ((), (), s32[]{:S(2)}) async-start(), calls=%async_computation.4 | async-start | bytes 1310720 | tf_op jit(solution)/shard_map/all_gather | solution.py:22
  187.3 59.3 %all-gather.25.cloned.1.call-start = ((), (), s32[]{:S(2)}) async-start(), calls=%async_computation.9 | async-start | bytes 1179648 | tf_op jit(solution)/shard_map/all_gather | solution.py:29
  188.0 99.7 %all-gather.27.cloned.1.call-start = ((), (), s32[]{:S(2)}) async-start(), calls=%async_computation.10 | async-start | bytes 1179648 | tf_op jit(solution)/shard_map/all_gather | solution.py:30
  188.8 139.1 %all-gather.29.cloned.1.call-start = ((), (), s32[]{:S(2)}) async-start(), calls=%async_computation.11 | async-start | bytes 1179648 | tf_op jit(solution)/shard_map/all_gather | solution.py:52
  189.5 171.9 %reduce-scatter.5.cloned.1.call-start = ((), (), s32[]{:S(2)}) async-start(), calls=%async_computation.5 | async-start | bytes 2621440 | tf_op jit(solution)/shard_map/reduce_scatter | solution.py:54
  204.1 83.6 %copy-start.2 = (bf16[256,2048]{1,0:T(8,128)(2,1)S(1)}, bf16[256,2048]{1,0:T(8,128)(2,1)}, u32[]{:S(2)}) copy-start(bf16[256,2048]{1,0:T(8,128)(2,1)} %all-gather.17.cloned.1.call-done) | copy-start | bytes 3145732
  289.5 4.4 %collective-permute-start.1 = (bf16[128,256]{1,0:T(8,128)(2,1)S(1)}, bf16[128,256]{1,0:T(8,128)(2,1)S(1)}, u32[]{:S(2)}, u32[]{:S(2)}) collective-permute-start(bf16[128,256]{1,0:T(8,128)(2,1)S(1)} %slice.66), channel_id=1, source_target_pairs={{0,4},{4,8},{8,12},{12,16},{16,20},{20,24},{24,28},{1,5},{5,9},{9,... | collective-permute-start | bytes 196616 | tf_op jit(solution)/shard_map/ppermute | solution.py:13
  327.9 33.5 %copy-start = (bf16[256,512]{1,0:T(8,128)(2,1)S(1)}, bf16[256,512]{1,0:T(8,128)(2,1)}, u32[]{:S(2)}) copy-start(bf16[256,512]{1,0:T(8,128)(2,1)} %add_convert_fusion.1) | copy-start | bytes 786436
Sparse Core Ops, SparseCore 0:
  8.9 19.4 all-gather.14
  30.5 40.2 all-gather.18
  72.9 38.9 all-gather.20
  113.8 38.0 all-gather.22
  155.2 30.1 reduce-scatter.2
  187.4 16.6 all-gather.16
  206.3 40.2 all-gather.24
  248.7 38.9 all-gather.26
  289.8 38.0 all-gather.28
  331.2 30.1 reduce-scatter.4
where the time goes:
time: 371 us; the launch traced here: 370 us
  waiting for transfers between devices  290 us (78%)
  blocking collectives  25.3 us (7%)
  matrix products  23.4 us (6%)
  between operations  13.7 us (4%)
  other arithmetic  7.31 us (2%)
  starting transfers between devices  5.32 us (1%)
  local copies, waits for them, and re-layouts  5.19 us (1%)
    all_gather x2, waiting for transfers between devices, shards(): lax.all_gather(w_value[layer], 'sp', axis=0, tiled=True)  81.7 us
    all_gather x2, waiting for transfers between devices, shards(): lax.all_gather(w_gate[layer], 'sp', axis=0, tiled=True)  78.2 us
    reduce_scatter x2, waiting for transfers between devices, shards(): branch = lax.psum_scatter(terms, 'tp', scatter_dimension=1, tiled=True)  60.6 us
    all_gather x2, waiting for transfers between devices, shards(): out_whole = lax.all_gather(w_out[layer], 'sp', axis=1, tiled=True)  32.5 us
    all_gather x2, waiting for transfers between devices, shards(): whole = lax.all_gather(x, 'tp', axis=1, tiled=True).astype(jnp.float32)  30.3 us
    psum x2, blocking collectives, shards(): lax.psum(jnp.sum(centred * centred, axis=1, keepdims=True), 'tp') / C  14 us
    psum x2, blocking collectives, shards(): mean = lax.psum(jnp.sum(conv, axis=1, keepdims=True), 'tp') / C  11.3 us
    conv_general_dilated x2, matrix products, shards(): lax.conv_general_dilated(padded[None], conv_taps[layer][:, None, :], (1,)...  9.67 us
  transfers between devices with their start and end apart: 12, of which 12 were waited for; matrix products, arithmetic and copies ran while one was open for 7% of the time, Pallas kernels for 0%

commit v1 on v0

--- a/solution.py
+++ b/solution.py
@@ -5,6 +5,19 @@
 
 C = 1024
 LAYERS = 2
+
+
+def mix_chains_over_axis(body):
+    cores_n = lax.axis_size("sp")
+    pool = [(tick, (tick + 1) % cores_n) for tick in range(cores_n)]
+    block_out = [None] * cores_n
+    block_out[cores_n - 1] = body
+    for pp in range(cores_n - 2, -1, -1):
+        block_out[pp] = lax.ppermute(block_out[pp + 1], axis_name="sp", perm=pool)
+    formed = jnp.concatenate(block_out, axis=1)
+    state_next = lax.axis_index("sp")
+    long_array = (state_next + 1) * body.shape[1]
+    return jnp.roll(formed, shift=long_array, axis=1)
 
 
 def from_behind(value, axis, steps):
@@ -49,7 +62,7 @@
         act = jax.nn.silu(centred * lax.rsqrt(spread + 1e-05) * channel_gain[layer]).astype(
             jnp.bfloat16
         )
-        out_whole = lax.all_gather(w_out[layer], "sp", axis=1, tiled=True)
+        out_whole = mix_chains_over_axis(w_out[layer])
         terms = jnp.dot(act, out_whole, preferred_element_type=jnp.float32)
         branch = lax.psum_scatter(terms, "tp", scatter_dimension=1, tiled=True)
         x = (x.astype(jnp.float32) + branch).astype(jnp.bfloat16)

time: 371 us -> 347 us (0.935)
  waiting for transfers between devices: 290 us -> 258 us
  local copies, waits for them, and re-layouts: 5.19 us -> 9.99 us
  starting transfers between devices: 5.32 us -> 9.83 us
    ppermute x0 -> x14, waiting for transfers between devices: none -> 64.5 us  [mix_chains_over_axis(): block_out[pp] = lax.ppermute(block_out[pp + 1], axis_name='sp', perm=pool)]
    all_gather x2, waiting for transfers between devices: 81.7 us -> 40.7 us  [shards(): lax.all_gather(w_value[layer], 'sp', axis=0, tiled=True)]
    all_gather x2 -> x0, waiting for transfers between devices: 32.5 us -> none  [shards(): out_whole = lax.all_gather(w_out[layer], 'sp', axis=1, tiled=True)]
    all_gather x2, waiting for transfers between devices: 30.3 us -> 15.5 us  [shards(): whole = lax.all_gather(x, 'tp', axis=1, tiled=True).astype(jnp.float32)]
    all_gather x2, waiting for transfers between devices: 78.2 us -> 68.2 us  [shards(): lax.all_gather(w_gate[layer], 'sp', axis=0, tiled=True)]
    unnamed x14 -> x30, local copies, waits for them, and re-layouts: 0.03 us -> 4.86 us
    ppermute x0 -> x14, starting transfers between devices: none -> 4.6 us  [mix_chains_over_axis(): block_out[pp] = lax.ppermute(block_out[pp + 1], axis_name='sp', perm=pool)]
  transfers between devices with their start and end apart: 12 -> 24, of which waited for: 12 -> 22; matrix products, arithmetic and copies ran while one was open for 7% -> 5% of each run, Pallas kernels for 0% -> 0%
where the time goes in v1:
time: 347 us; the launch traced here: 346 us
  waiting for transfers between devices  258 us (74%)
  blocking collectives  24.5 us (7%)
  matrix products  22.6 us (7%)
  between operations  13.7 us (4%)
  local copies, waits for them, and re-layouts  9.99 us (3%)
  starting transfers between devices  9.83 us (3%)
  other arithmetic  7.32 us (2%)
    all_gather x2, waiting for transfers between devices, shards(): lax.all_gather(w_gate[layer], 'sp', axis=0, tiled=True)  68.2 us
    ppermute x14, waiting for transfers between devices, mix_chains_over_axis(): block_out[pp] = lax.ppermute(block_out[pp + 1], axis_name='sp', perm=pool)  64.5 us
    reduce_scatter x2, waiting for transfers between devices, shards(): branch = lax.psum_scatter(terms, 'tp', scatter_dimension=1, tiled=True)  64.2 us
    all_gather x2, waiting for transfers between devices, shards(): lax.all_gather(w_value[layer], 'sp', axis=0, tiled=True)  40.7 us
    all_gather x2, waiting for transfers between devices, shards(): whole = lax.all_gather(x, 'tp', axis=1, tiled=True).astype(jnp.float32)  15.5 us
    psum x2, blocking collectives, shards(): lax.psum(jnp.sum(centred * centred, axis=1, keepdims=True), 'tp') / C  13.2 us
    psum x2, blocking collectives, shards(): mean = lax.psum(jnp.sum(conv, axis=1, keepdims=True), 'tp') / C  11.3 us
    conv_general_dilated x2, matrix products, shards(): lax.conv_general_dilated(padded[None], conv_taps[layer][:, None, :], (1,)...  9.67 us
  transfers between devices with their start and end apart: 24, of which 22 were waited for; matrix products, arithmetic and copies ran while one was open for 5% of the time, Pallas kernels for 0%

profile of v1, /device:TPU:0, one launch (start us, length us, event | category | flops | bytes accessed | tf_op | source)
XLA Modules:
  0.0 346.1 jit_solution(10852301936190354861)
XLA Ops:
  14.6 5.9 %collective-permute-done.9 = bf16[256,256]{1,0:T(8,128)(2,1)S(1)} collective-permute-done((bf16[256,256]{1,0:T(8,128)(2,1)S(1)}, bf16[256,256]{1,0:T(8,128)(2,1)S(1)}, u32[]{:S(2)}, u32[]{:S(2)}) %collective-permute-start.9) | collective-permute-done | bytes 131104 | tf_op jit(solution)/shard_map/ppermute | solution.py:16
  22.4 6.9 %collective-permute-done.10 = bf16[256,256]{1,0:T(8,128)(2,1)S(1)} collective-permute-done((bf16[256,256]{1,0:T(8,128)(2,1)S(1)}, bf16[256,256]{1,0:T(8,128)(2,1)S(1)}, u32[]{:S(2)}, u32[]{:S(2)}) %collective-permute-start.10) | collective-permute-done | bytes 131104 | tf_op jit(solution)/shard_map/ppermute | solution.py:16
  31.2 7.1 %collective-permute-done.11 = bf16[256,256]{1,0:T(8,128)(2,1)S(1)} collective-permute-done((bf16[256,256]{1,0:T(8,128)(2,1)S(1)}, bf16[256,256]{1,0:T(8,128)(2,1)S(1)}, u32[]{:S(2)}, u32[]{:S(2)}) %collective-permute-start.11) | collective-permute-done | bytes 131104 | tf_op jit(solution)/shard_map/ppermute | solution.py:16
  40.8 9.0 %collective-permute-done.12 = bf16[256,256]{1,0:T(8,128)(2,1)S(1)} collective-permute-done((bf16[256,256]{1,0:T(8,128)(2,1)S(1)}, bf16[256,256]{1,0:T(8,128)(2,1)S(1)}, u32[]{:S(2)}, u32[]{:S(2)}) %collective-permute-start.12) | collective-permute-done | bytes 131104 | tf_op jit(solution)/shard_map/ppermute | solution.py:16
  49.9 4.0 %collective-permute-done.4 = bf16[256,256]{1,0:T(8,128)(2,1)S(1)} collective-permute-done((bf16[256,256]{1,0:T(8,128)(2,1)S(1)}, bf16[256,256]{1,0:T(8,128)(2,1)S(1)}, u32[]{:S(2)}, u32[]{:S(2)}) %collective-permute-start.4) | collective-permute-done | bytes 131104 | tf_op jit(solution)/shard_map/ppermute | solution.py:16
  53.9 4.6 %collective-permute-done.13 = bf16[256,256]{1,0:T(8,128)(2,1)S(1)} collective-permute-done((bf16[256,256]{1,0:T(8,128)(2,1)S(1)}, bf16[256,256]{1,0:T(8,128)(2,1)S(1)}, u32[]{:S(2)}, u32[]{:S(2)}) %collective-permute-start.13) | collective-permute-done | bytes 131104 | tf_op jit(solution)/shard_map/ppermute | solution.py:16
  58.5 3.9 %collective-permute-done.5 = bf16[256,256]{1,0:T(8,128)(2,1)S(1)} collective-permute-done((bf16[256,256]{1,0:T(8,128)(2,1)S(1)}, bf16[256,256]{1,0:T(8,128)(2,1)S(1)}, u32[]{:S(2)}, u32[]{:S(2)}) %collective-permute-start.5) | collective-permute-done | bytes 131104 | tf_op jit(solution)/shard_map/ppermute | solution.py:16
  62.4 7.6 %collective-permute-done.14 = bf16[256,256]{1,0:T(8,128)(2,1)S(1)} collective-permute-done((bf16[256,256]{1,0:T(8,128)(2,1)S(1)}, bf16[256,256]{1,0:T(8,128)(2,1)S(1)}, u32[]{:S(2)}, u32[]{:S(2)}) %collective-permute-start.14) | collective-permute-done | bytes 131104 | tf_op jit(solution)/shard_map/ppermute | solution.py:16
  70.1 3.4 collective-permute-done.6
  73.5 4.3 %collective-permute-done.15 = bf16[256,256]{1,0:T(8,128)(2,1)S(1)} collective-permute-done((bf16[256,256]{1,0:T(8,128)(2,1)S(1)}, bf16[256,256]{1,0:T(8,128)(2,1)S(1)}, u32[]{:S(2)}, u32[]{:S(2)}) %collective-permute-start.15) | collective-permute-done | bytes 131104 | tf_op jit(solution)/shard_map/ppermute | solution.py:16
  78.0 3.2 collective-permute-done.7
  89.7 29.1 %all-gather.17.cloned.1.call-done = bf16[1,2048,256]{2,1,0:T(8,128)(2,1)} async-done(((bf16[1,256,256]{2,1,0:T(8,128)(2,1)}), bf16[1,2048,256]{2,1,0:T(8,128)(2,1)}) %all-gather.17.cloned.1.call-update) | async-done | bytes 1048592 | tf_op jit(solution)/shard_map/all_gather | solution.py:43
  124.9 4.8 %fusion.55 = (f32[256]{0:T(256)S(1)}, f32[1,256,256]{2,0,1:T(1,128)S(1)}) fusion(f32[1,128,256]{2,1,0:T(8,128)S(1)} %get-tuple-element.7, bf16[1,383,256]{2,1,0:T(8,128)(2,1)S(1)} %maximum_bitcast_fusion), kind=kOutput, calls=%fused_computation.95 | convolution fusion | flops 100728576 | bytes 590336 | tf_op jit(solution)/shard_map/conv_general_dilated | solution.py:50
  129.7 5.7 %psum.28 = f32[256,1]{0,1:T(1,128)S(1)} all-reduce(f32[256,1]{0,1:T(1,128)S(1)} %bitcast.72), channel_id=1, replica_groups=mesh['sp'=8,'tp'=4] {'tp'}, use_global_device_ids=true, to_apply=%region_2.0 | all-reduce | flops 256 | bytes 2048 | tf_op jit(solution)/shard_map/psum | solution.py:59
  135.6 6.6 %psum.29 = f32[256,1]{0,1:T(1,128)S(1)} all-reduce(f32[256,1]{0,1:T(1,128)S(1)} %bitcast.68), channel_id=1, replica_groups=mesh['sp'=8,'tp'=4] {'tp'}, use_global_device_ids=true, to_apply=%region_4.0 | all-reduce | flops 256 | bytes 2048 | tf_op jit(solution)/shard_map/psum | solution.py:61
  142.2 3.3 fusion.20
  145.6 32.0 %reduce-scatter.3.cloned.1.call-done = f32[256,512]{1,0:T(8,128)} async-done(((f32[256,2048]{1,0:T(8,128)}), f32[256,512]{1,0:T(8,128)}) %reduce-scatter.3.cloned.1.call-update) | async-done | bytes 524304 | tf_op jit(solution)/shard_map/reduce_scatter | solution.py:67
  180.8 15.5 %all-gather.13.cloned.1.call-done = bf16[256,2048]{1,0:T(8,128)(2,1)} async-done(((bf16[256,512]{1,0:T(8,128)(2,1)}), bf16[256,2048]{1,0:T(8,128)(2,1)}) %all-gather.13.cloned.1.call-update) | async-done | bytes 1048592 | tf_op jit(solution)/shard_map/all_gather | solution.py:35
  197.9 40.7 %all-gather.19.cloned.1.call-done = bf16[1,2048,256]{2,1,0:T(8,128)(2,1)} async-done(((bf16[1,256,256]{2,1,0:T(8,128)(2,1)}), bf16[1,2048,256]{2,1,0:T(8,128)(2,1)}) %all-gather.19.cloned.1.call-update) | async-done | bytes 1048592 | tf_op jit(solution)/shard_map/all_gather | solution.py:42
  240.6 39.1 %all-gather.21.cloned.1.call-done = bf16[1,2048,256]{2,1,0:T(8,128)(2,1)} async-done(((bf16[1,256,256]{2,1,0:T(8,128)(2,1)}), bf16[1,2048,256]{2,1,0:T(8,128)(2,1)}) %all-gather.21.cloned.1.call-update) | async-done | bytes 1048592 | tf_op jit(solution)/shard_map/all_gather | solution.py:43
  285.9 4.8 %fusion.56 = (f32[256]{0:T(256)S(1)}, f32[1,256,256]{2,0,1:T(1,128)S(1)}) fusion(f32[1,128,256]{2,1,0:T(8,128)S(1)} %get-tuple-element.6, bf16[1,383,256]{2,1,0:T(8,128)(2,1)S(1)} %maximum_bitcast_fusion.1), kind=kOutput, calls=%fused_computation.96 | convolution fusion | flops 100728576 | bytes 590336 | tf_op jit(solution)/shard_map/conv_general_dilated | solution.py:50
  290.7 5.7 %psum.30 = f32[256,1]{0,1:T(1,128)S(1)} all-reduce(f32[256,1]{0,1:T(1,128)S(1)} %bitcast.73), channel_id=1, replica_groups=mesh['sp'=8,'tp'=4] {'tp'}, use_global_device_ids=true, to_apply=%region_8.10 | all-reduce | flops 256 | bytes 2048 | tf_op jit(solution)/shard_map/psum | solution.py:59
  296.6 6.6 %psum.31 = f32[256,1]{0,1:T(1,128)S(1)} all-reduce(f32[256,1]{0,1:T(1,128)S(1)} %bitcast.69), channel_id=1, replica_groups=mesh['sp'=8,'tp'=4] {'tp'}, use_global_device_ids=true, to_apply=%region_10.12 | all-reduce | flops 256 | bytes 2048 | tf_op jit(solution)/shard_map/psum | solution.py:61
  305.3 32.1 %reduce-scatter.5.cloned.1.call-done = f32[256,512]{1,0:T(8,128)} async-done(((f32[256,2048]{1,0:T(8,128)}), f32[256,512]{1,0:T(8,128)}) %reduce-scatter.5.cloned.1.call-update) | async-done | bytes 524304 | tf_op jit(solution)/shard_map/reduce_scatter | solution.py:67
  (99 shorter events, 46.4 us)
Async XLA Ops:
  6.5 79.4 %all-gather.11.cloned.1.call-start = ((), (), s32[]{:S(2)}) async-start(), calls=%async_computation.2 | async-start | bytes 1310720 | tf_op jit(solution)/shard_map/all_gather | solution.py:35
  7.3 80.3 %all-gather.15.cloned.1.call-start = ((), (), s32[]{:S(2)}) async-start(), calls=%async_computation.6 | async-start | bytes 1179648 | tf_op jit(solution)/shard_map/all_gather | solution.py:42
  9.0 109.7 %all-gather.17.cloned.1.call-start = ((), (), s32[]{:S(2)}) async-start(), calls=%async_computation.7 | async-start | bytes 1179648 | tf_op jit(solution)/shard_map/all_gather | solution.py:43
  10.1 10.4 %collective-permute-start.9 = (bf16[256,256]{1,0:T(8,128)(2,1)S(1)}, bf16[256,256]{1,0:T(8,128)(2,1)S(1)}, u32[]{:S(2)}, u32[]{:S(2)}) collective-permute-start(bf16[256,256]{1,0:T(8,128)(2,1)S(1)} %get-tuple-element.15), channel_id=1, source_target_pairs={{0,4},{4,8},{8,12},{12,16},{16,20},{20,24},{24,28},{28,0},{1,5},{5... | collective-permute-start | bytes 393224 | tf_op jit(solution)/shard_map/ppermute | solution.py:16
  13.1 9.3 %collective-permute-start.1 = (bf16[256,256]{1,0:T(8,128)(2,1)S(1)}, bf16[256,256]{1,0:T(8,128)(2,1)S(1)}, u32[]{:S(2)}, u32[]{:S(2)}) collective-permute-start(bf16[256,256]{1,0:T(8,128)(2,1)S(1)} %get-tuple-element.14), channel_id=1, source_target_pairs={{0,4},{4,8},{8,12},{12,16},{16,20},{20,24},{24,28},{28,0},{1,5},{5... | collective-permute-start | bytes 393224 | tf_op jit(solution)/shard_map/ppermute | solution.py:16
  20.5 8.8 %collective-permute-start.10 = (bf16[256,256]{1,0:T(8,128)(2,1)S(1)}, bf16[256,256]{1,0:T(8,128)(2,1)S(1)}, u32[]{:S(2)}, u32[]{:S(2)}) collective-permute-start(bf16[256,256]{1,0:T(8,128)(2,1)S(1)} %collective-permute-done.9), channel_id=1, source_target_pairs={{0,4},{4,8},{8,12},{12,16},{16,20},{20,24},{24,28},{28,0},{1,5},{5... | collective-permute-start | bytes 393224 | tf_op jit(solution)/shard_map/ppermute | solution.py:16
  22.4 8.8 %collective-permute-start.2 = (bf16[256,256]{1,0:T(8,128)(2,1)S(1)}, bf16[256,256]{1,0:T(8,128)(2,1)S(1)}, u32[]{:S(2)}, u32[]{:S(2)}) collective-permute-start(bf16[256,256]{1,0:T(8,128)(2,1)S(1)} %collective-permute-done.1), channel_id=1, source_target_pairs={{0,4},{4,8},{8,12},{12,16},{16,20},{20,24},{24,28},{28,0},{1,5},{5... | collective-permute-start | bytes 393224 | tf_op jit(solution)/shard_map/ppermute | solution.py:16
  29.3 9.1 %collective-permute-start.11 = (bf16[256,256]{1,0:T(8,128)(2,1)S(1)}, bf16[256,256]{1,0:T(8,128)(2,1)S(1)}, u32[]{:S(2)}, u32[]{:S(2)}) collective-permute-start(bf16[256,256]{1,0:T(8,128)(2,1)S(1)} %collective-permute-done.10), channel_id=1, source_target_pairs={{0,4},{4,8},{8,12},{12,16},{16,20},{20,24},{24,28},{28,0},{1,5},{5... | collective-permute-start | bytes 393224 | tf_op jit(solution)/shard_map/ppermute | solution.py:16
  31.2 9.6 %collective-permute-start.3 = (bf16[256,256]{1,0:T(8,128)(2,1)S(1)}, bf16[256,256]{1,0:T(8,128)(2,1)S(1)}, u32[]{:S(2)}, u32[]{:S(2)}) collective-permute-start(bf16[256,256]{1,0:T(8,128)(2,1)S(1)} %collective-permute-done.2), channel_id=1, source_target_pairs={{0,4},{4,8},{8,12},{12,16},{16,20},{20,24},{24,28},{28,0},{1,5},{5... | collective-permute-start | bytes 393224 | tf_op jit(solution)/shard_map/ppermute | solution.py:16
  38.4 11.5 %collective-permute-start.12 = (bf16[256,256]{1,0:T(8,128)(2,1)S(1)}, bf16[256,256]{1,0:T(8,128)(2,1)S(1)}, u32[]{:S(2)}, u32[]{:S(2)}) collective-permute-start(bf16[256,256]{1,0:T(8,128)(2,1)S(1)} %collective-permute-done.11), channel_id=1, source_target_pairs={{0,4},{4,8},{8,12},{12,16},{16,20},{20,24},{24,28},{28,0},{1,5},{5... | collective-permute-start | bytes 393224 | tf_op jit(solution)/shard_map/ppermute | solution.py:16
  40.1 137.5 %reduce-scatter.3.cloned.1.call-start = ((), (), s32[]{:S(2)}) async-start(), calls=%async_computation.3 | async-start | bytes 2621440 | tf_op jit(solution)/shard_map/reduce_scatter | solution.py:67
  40.8 13.1 %collective-permute-start.4 = (bf16[256,256]{1,0:T(8,128)(2,1)S(1)}, bf16[256,256]{1,0:T(8,128)(2,1)S(1)}, u32[]{:S(2)}, u32[]{:S(2)}) collective-permute-start(bf16[256,256]{1,0:T(8,128)(2,1)S(1)} %collective-permute-done.3), channel_id=1, source_target_pairs={{0,4},{4,8},{8,12},{12,16},{16,20},{20,24},{24,28},{28,0},{1,5},{5... | collective-permute-start | bytes 393224 | tf_op jit(solution)/shard_map/ppermute | solution.py:16
  49.9 8.6 %collective-permute-start.13 = (bf16[256,256]{1,0:T(8,128)(2,1)S(1)}, bf16[256,256]{1,0:T(8,128)(2,1)S(1)}, u32[]{:S(2)}, u32[]{:S(2)}) collective-permute-start(bf16[256,256]{1,0:T(8,128)(2,1)S(1)} %collective-permute-done.12), channel_id=1, source_target_pairs={{0,4},{4,8},{8,12},{12,16},{16,20},{20,24},{24,28},{28,0},{1,5},{5... | collective-permute-start | bytes 393224 | tf_op jit(solution)/shard_map/ppermute | solution.py:16
  53.9 8.6 %collective-permute-start.5 = (bf16[256,256]{1,0:T(8,128)(2,1)S(1)}, bf16[256,256]{1,0:T(8,128)(2,1)S(1)}, u32[]{:S(2)}, u32[]{:S(2)}) collective-permute-start(bf16[256,256]{1,0:T(8,128)(2,1)S(1)} %collective-permute-done.4), channel_id=1, source_target_pairs={{0,4},{4,8},{8,12},{12,16},{16,20},{20,24},{24,28},{28,0},{1,5},{5... | collective-permute-start | bytes 393224 | tf_op jit(solution)/shard_map/ppermute | solution.py:16
  58.5 11.6 %collective-permute-start.14 = (bf16[256,256]{1,0:T(8,128)(2,1)S(1)}, bf16[256,256]{1,0:T(8,128)(2,1)S(1)}, u32[]{:S(2)}, u32[]{:S(2)}) collective-permute-start(bf16[256,256]{1,0:T(8,128)(2,1)S(1)} %collective-permute-done.13), channel_id=1, source_target_pairs={{0,4},{4,8},{8,12},{12,16},{16,20},{20,24},{24,28},{28,0},{1,5},{5... | collective-permute-start | bytes 393224 | tf_op jit(solution)/shard_map/ppermute | solution.py:16
  62.4 11.1 %collective-permute-start.6 = (bf16[256,256]{1,0:T(8,128)(2,1)S(1)}, bf16[256,256]{1,0:T(8,128)(2,1)S(1)}, u32[]{:S(2)}, u32[]{:S(2)}) collective-permute-start(bf16[256,256]{1,0:T(8,128)(2,1)S(1)} %collective-permute-done.5), channel_id=1, source_target_pairs={{0,4},{4,8},{8,12},{12,16},{16,20},{20,24},{24,28},{28,0},{1,5},{5... | collective-permute-start | bytes 393224 | tf_op jit(solution)/shard_map/ppermute | solution.py:16
  70.1 7.8 %collective-permute-start.15 = (bf16[256,256]{1,0:T(8,128)(2,1)S(1)}, bf16[256,256]{1,0:T(8,128)(2,1)S(1)}, u32[]{:S(2)}, u32[]{:S(2)}) collective-permute-start(bf16[256,256]{1,0:T(8,128)(2,1)S(1)} %collective-permute-done.14), channel_id=1, source_target_pairs={{0,4},{4,8},{8,12},{12,16},{16,20},{20,24},{24,28},{28,0},{1,5},{5... | collective-permute-start | bytes 393224 | tf_op jit(solution)/shard_map/ppermute | solution.py:16
  73.5 7.7 %collective-permute-start.7 = (bf16[256,256]{1,0:T(8,128)(2,1)S(1)}, bf16[256,256]{1,0:T(8,128)(2,1)S(1)}, u32[]{:S(2)}, u32[]{:S(2)}) collective-permute-start(bf16[256,256]{1,0:T(8,128)(2,1)S(1)} %collective-permute-done.6), channel_id=1, source_target_pairs={{0,4},{4,8},{8,12},{12,16},{16,20},{20,24},{24,28},{28,0},{1,5},{5... | collective-permute-start | bytes 393224 | tf_op jit(solution)/shard_map/ppermute | solution.py:16
  120.5 4.4 %collective-permute-start = (bf16[128,256]{1,0:T(8,128)(2,1)S(1)}, bf16[128,256]{1,0:T(8,128)(2,1)S(1)}, u32[]{:S(2)}, u32[]{:S(2)}) collective-permute-start(bf16[128,256]{1,0:T(8,128)(2,1)S(1)} %slice.64), channel_id=1, source_target_pairs={{0,4},{4,8},{8,12},{12,16},{16,20},{20,24},{24,28},{1,5},{5,9},{9,... | collective-permute-start | bytes 196616 | tf_op jit(solution)/shard_map/ppermute | solution.py:26
  145.5 50.8 %all-gather.13.cloned.1.call-start = ((), (), s32[]{:S(2)}) async-start(), calls=%async_computation.4 | async-start | bytes 1310720 | tf_op jit(solution)/shard_map/all_gather | solution.py:35
  179.4 59.1 %all-gather.19.cloned.1.call-start = ((), (), s32[]{:S(2)}) async-start(), calls=%async_computation.8 | async-start | bytes 1179648 | tf_op jit(solution)/shard_map/all_gather | solution.py:42
  180.0 99.7 %all-gather.21.cloned.1.call-start = ((), (), s32[]{:S(2)}) async-start(), calls=%async_computation.9 | async-start | bytes 1179648 | tf_op jit(solution)/shard_map/all_gather | solution.py:43
  180.8 156.7 %reduce-scatter.5.cloned.1.call-start = ((), (), s32[]{:S(2)}) async-start(), calls=%async_computation.5 | async-start | bytes 2621440 | tf_op jit(solution)/shard_map/reduce_scatter | solution.py:67
  281.5 4.4 %collective-permute-start.8 = (bf16[128,256]{1,0:T(8,128)(2,1)S(1)}, bf16[128,256]{1,0:T(8,128)(2,1)S(1)}, u32[]{:S(2)}, u32[]{:S(2)}) collective-permute-start(bf16[128,256]{1,0:T(8,128)(2,1)S(1)} %slice.66), channel_id=1, source_target_pairs={{0,4},{4,8},{8,12},{12,16},{16,20},{20,24},{24,28},{1,5},{5,9},{9,... | collective-permute-start | bytes 196616 | tf_op jit(solution)/shard_map/ppermute | solution.py:26
  (8 other events, 372.6 us)
Sparse Core Ops, SparseCore 0:
  8.9 19.4 all-gather.10
  30.5 46.4 all-gather.14
  79.1 39.5 all-gather.16
  145.6 31.9 reduce-scatter.2
  179.6 16.6 all-gather.12
  198.3 40.2 all-gather.18
  240.7 38.9 all-gather.20
  305.4 31.9 reduce-scatter.4
